TPU v7x, 32 devices: a whole 2x2x4 slice. The times are simulated.
32 devices in a mesh: pp: 4 (over y, x), fs: 4 (over z), tp: 2 (over core).
Axes of the slice: x: 2, y: 2, z: 4, core: 2. Of those that a mesh axis runs over, the one named last changes fastest.
Arguments:
- micro_in: bfloat16 [2, 96, 1024], P(None, 'pp', ('tp', 'fs')), may hold values from -6 to 6
- norm_gain: float32 [4, 1024], P('pp'), may hold values from 0.5 to 1.5
- proj_gate: bfloat16 [4, 1024, 8, 4, 64], P('pp', None, 'tp', 'fs'), may hold values from -0.1875 to 0.1875
- proj_value: bfloat16 [4, 1024, 8, 4, 64], P('pp', None, 'tp', 'fs'), may hold values from -0.1875 to 0.1875
- proj_write: bfloat16 [4, 1024, 8, 128], P('pp', None, 'tp'), may hold values from -0.1875 to 0.1875
- proj_read: bfloat16 [4, 1024, 8, 128], P('pp', None, 'tp'), may hold values from -0.1875 to 0.1875
- proj_step: bfloat16 [4, 1024, 2, 8, 4], P('pp', None, None, 'tp', 'fs'), may hold values from -0.1875 to 0.1875
- step_bias: float32 [4, 2, 8, 4], P('pp', None, 'tp', 'fs'), may hold values from -4.6 to -2.3
- decay_log: float32 [4, 2, 8, 4], P('pp', None, 'tp', 'fs'), may hold values from 0 to 2.77
- skip_gain: float32 [4, 8, 4], P('pp', 'tp', 'fs'), may hold values from 0.5 to 1.5
- conv_value: float32 [4, 5, 8, 4, 64], P('pp', None, 'tp', 'fs'), may hold values from -2.5 to 2.5
- conv_write: float32 [4, 5, 8, 128], P('pp', None, 'tp'), may hold values from -2.5 to 2.5
- conv_read: float32 [4, 5, 8, 128], P('pp', None, 'tp'), may hold values from -2.5 to 2.5
- proj_out: bfloat16 [4, 8, 4, 64, 1024], P('pp', 'tp', 'fs'), may hold values from -0.125 to 0.125
Outputs:
- mixed_out: bfloat16 [2, 96, 1024], P(None, 'pp', ('tp', 'fs'))
All inputs are finite; a program needn't handle non-finite values.
Results may differ from a plain program's by a relative error of at most 0.025.
Values may be sent and summed in bfloat16 or wider, within the bound.
A program may use at most 64 MiB of HBM per device.

v0:
```python
import jax
import jax.numpy as jnp
from jax import lax
from jax.sharding import PartitionSpec as P

epsilon = 1e-06


def own_rows_2(portion, span, axis):
    count = span * lax.axis_size(axis)
    sent = portion(jnp.int32(0), count).astype(jnp.bfloat16)
    return lax.psum_scatter(sent, axis, scatter_dimension=0, tiled=True).astype(jnp.float32)


def from_behind(block, axis, distance):
    devices = range(lax.axis_size(axis))
    route = [(i - distance, i) for i in devices if i - distance in devices]
    return lax.ppermute(block, axis, route)


def spread(value, axis, source):
    kept = jnp.where(lax.axis_index(axis) == source, value, 0).astype(value.dtype)
    return lax.psum(kept, axis)


def centred_conv(signal, conv_taps):
    span_width = conv_taps.shape[0]
    half_width = span_width // 2
    length = signal.shape[0]
    padded = jnp.pad(signal, ((half_width, half_width), (0, 0)))
    running = jnp.zeros_like(signal)
    for offset in range(span_width):
        running = running + padded[offset : offset + length] * conv_taps[offset]
    return running


def duality_mix(
    gate_flat,
    value_flat,
    write_flat,
    read_flat,
    step_raw,
    step_bias,
    decay_log,
    skip_gain,
    conv_value,
    conv_write,
    conv_read,
):
    groups, per_group = skip_gain.shape
    length = gate_flat.shape[0]
    head_size = value_flat.shape[1] // (groups * per_group)
    state_size = write_flat.shape[1] // groups
    taps_count = conv_value.shape[0]
    value_act = jax.nn.silu(
        centred_conv(value_flat.astype(jnp.float32), conv_value.reshape(taps_count, -1))
    ).astype(jnp.bfloat16)
    write_act = jax.nn.silu(
        centred_conv(write_flat.astype(jnp.float32), conv_write.reshape(taps_count, -1))
    ).astype(jnp.bfloat16)
    read_act = jax.nn.silu(
        centred_conv(read_flat.astype(jnp.float32), conv_read.reshape(taps_count, -1))
    ).astype(jnp.bfloat16)
    step_size = jax.nn.softplus(step_raw.reshape(length, 2, groups, per_group) + step_bias[None])
    log_decay = step_size * (-jnp.exp(decay_log))[None]
    fwd_cum = jnp.cumsum(log_decay[:, 0], axis=0)
    bwd_cum = jnp.flip(jnp.cumsum(jnp.flip(log_decay[:, 1], 0), axis=0), 0)
    positions = jnp.arange(length)
    lower_mask = (positions[:, None] >= positions[None, :])[:, :, None, None]
    upper_mask = (positions[:, None] <= positions[None, :])[:, :, None, None]
    fwd_weight = (
        jnp.exp(jnp.where(lower_mask, fwd_cum[:, None] - fwd_cum[None, :], -jnp.inf))
        * step_size[None, :, 0]
    )
    bwd_weight = (
        jnp.exp(jnp.where(upper_mask, bwd_cum[:, None] - bwd_cum[None, :], -jnp.inf))
        * step_size[None, :, 1]
    )
    scores = jnp.einsum(
        "tgn,sgn->tsg",
        read_act.reshape(length, groups, state_size),
        write_act.reshape(length, groups, state_size),
        preferred_element_type=jnp.float32,
    )
    combined = scores[:, :, :, None] * (fwd_weight + bwd_weight)
    value_heads = value_act.reshape(length, groups, per_group, head_size).astype(jnp.float32)
    mixed_heads = jnp.einsum(
        "tsgh,sghp->tghp", combined, value_heads, precision=lax.Precision.HIGHEST
    )
    mixed_heads = mixed_heads + skip_gain[None, :, :, None] * value_heads
    return (mixed_heads.reshape(length, -1) * jax.nn.silu(gate_flat.astype(jnp.float32))).astype(
        jnp.bfloat16
    )


def body(
    micro_in,
    norm_gain,
    proj_gate,
    proj_value,
    proj_write,
    proj_read,
    proj_step,
    step_bias,
    decay_log,
    skip_gain,
    conv_value,
    conv_write,
    conv_read,
    proj_out,
):
    section_count = lax.axis_size("pp")
    section_idx = lax.axis_index("pp")
    width_model = norm_gain.shape[1]
    fed_blocks = lax.all_gather(micro_in, "pp", axis=1, tiled=True)
    micro_count = fed_blocks.shape[0]
    length = fed_blocks.shape[1]
    fed_columns = jnp.swapaxes(fed_blocks, 1, 2)
    gain_vec = norm_gain[0].astype(jnp.float32)
    cut_gate = proj_gate.shape[2] * proj_gate.shape[3] * proj_gate.shape[4]
    cut_write = proj_write.shape[2] * proj_write.shape[3]
    weight_all = jnp.concatenate(
        [
            proj_gate[0].reshape(width_model, -1),
            proj_value[0].reshape(width_model, -1),
            proj_write[0].reshape(width_model, -1),
            proj_read[0].reshape(width_model, -1),
            proj_step[0].reshape(width_model, -1),
        ],
        axis=1,
    )
    out_weights = proj_out[0].reshape(-1, width_model)
    own_rows = width_model // lax.axis_size(("tp", "fs"))

    def project(column_block):
        gathered = lax.all_gather(column_block, ("tp", "fs"), axis=0, tiled=True)
        as_float = gathered.astype(jnp.float32)
        scale_rms = lax.rsqrt(jnp.mean(as_float * as_float, axis=0) + epsilon)
        normed = (as_float * scale_rms[None, :] * gain_vec[:, None]).astype(jnp.bfloat16)
        return lax.dot_general(
            normed, weight_all, (((0,), (0,)), ((), ())), preferred_element_type=jnp.float32
        )

    def term_maker(token_rows):

        def term_rows(offset, span_count):
            weight_cols = lax.dynamic_slice_in_dim(out_weights, offset, span_count, 1)
            return lax.dot_general(
                weight_cols,
                token_rows,
                (((0,), (1,)), ((), ())),
                preferred_element_type=jnp.float32,
            )

        return term_rows

    def mix_block(column_block):
        projected = project(column_block)
        gate_flat = projected[:, :cut_gate].astype(jnp.bfloat16)
        value_flat = projected[:, cut_gate : 2 * cut_gate].astype(jnp.bfloat16)
        write_flat = projected[:, 2 * cut_gate : 2 * cut_gate + cut_write].astype(jnp.bfloat16)
        read_flat = projected[:, 2 * cut_gate + cut_write : 2 * cut_gate + 2 * cut_write].astype(
            jnp.bfloat16
        )
        step_raw = projected[:, 2 * cut_gate + 2 * cut_write :]
        gated_out = duality_mix(
            gate_flat,
            value_flat,
            write_flat,
            read_flat,
            step_raw,
            step_bias[0],
            decay_log[0],
            skip_gain[0],
            conv_value[0],
            conv_write[0],
            conv_read[0],
        )
        summed = own_rows_2(term_maker(gated_out), own_rows, ("tp", "fs"))
        branch = lax.optimization_barrier(summed.astype(jnp.bfloat16))
        return (column_block.astype(jnp.float32) + 0.5 * branch.astype(jnp.float32)).astype(
            jnp.bfloat16
        )

    total_steps = micro_count + section_count - 1

    def advance(moment, loop_state):
        arriving, collected = loop_state
        pick_index = jnp.clip(moment, 0, micro_count - 1)
        fresh_block = lax.dynamic_index_in_dim(fed_columns, pick_index, 0, keepdims=False)
        current = jnp.where(section_idx == 0, fresh_block, arriving)
        produced = mix_block(current)
        slot_index = moment - section_idx
        keep_flag = (
            (section_idx == section_count - 1) & (slot_index >= 0) & (slot_index < micro_count)
        )
        slot_safe = jnp.clip(slot_index, 0, micro_count - 1)
        previous = lax.dynamic_index_in_dim(collected, slot_safe, 0, keepdims=False)
        collected = lax.dynamic_update_index_in_dim(
            collected, jnp.where(keep_flag, produced, previous), slot_safe, 0
        )
        arriving = from_behind(produced, "pp", 1)
        return (arriving, collected)

    start_loop = (jnp.zeros_like(fed_columns[0]), jnp.zeros_like(fed_columns))
    arriving, collected = lax.fori_loop(0, total_steps, advance, start_loop)
    shared = spread(collected, "pp", section_count - 1)
    token_share = length // section_count
    own_block = lax.dynamic_slice_in_dim(shared, section_idx * token_share, token_share, 2)
    as_float = own_block.astype(jnp.float32)
    partial_squares = jnp.sum(as_float * as_float, axis=1)
    total_squares = lax.psum(partial_squares, ("tp", "fs"))
    scale_rms = lax.rsqrt(total_squares / width_model + epsilon)
    result = (as_float * scale_rms[:, None, :]).astype(jnp.bfloat16)
    return jnp.swapaxes(result, 1, 2)


def solution(mesh):
    return jax.shard_map(
        body,
        mesh=mesh,
        in_specs=(
            P(None, "pp", ("tp", "fs")),
            P("pp", None),
            P("pp", None, "tp", "fs", None),
            P("pp", None, "tp", "fs", None),
            P("pp", None, "tp", None),
            P("pp", None, "tp", None),
            P("pp", None, None, "tp", "fs"),
            P("pp", None, "tp", "fs"),
            P("pp", None, "tp", "fs"),
            P("pp", "tp", "fs"),
            P("pp", None, "tp", "fs", None),
            P("pp", None, "tp", None),
            P("pp", None, "tp", None),
            P("pp", "tp", "fs", None, None),
        ),
        out_specs=P(None, "pp", ("tp", "fs")),
        check_vma=False,
    )
```

profile of v0, /device:TPU:0, one launch (start us, length us, event | category | flops | bytes accessed | tf_op | source)
XLA Modules:
  0.0 515.9 jit_solution(10900077778748892538)
XLA Ops:
  6.5 2.0 copy.56
  8.6 1.1 constant_dynamic-update-slice_fusion.2
  9.7 2.0 copy.57
  11.7 1.2 constant_dynamic-update-slice_fusion.1
  12.9 1.4 bitcast_dynamic-update-slice_fusion.2
  16.3 10.4 %all_gather.13 = bf16[2,96,128]{2,1,0:T(8,128)(2,1)} all-gather(bf16[2,24,128]{2,1,0:T(8,128)(2,1)S(1)} %copy-done.6), channel_id=1, replica_groups=mesh['pp'=4,'fs'=4,'tp'=2] {'pp'}, dimensions={1}, use_global_device_ids=true | all-gather | bytes 61440 | tf_op jit(solution)/shard_map/all_gather | solution.py:115
  27.9 448.8 %while.17 = (s32[]{:T(128)}, bf16[128,96]{0,1:T(8,128)(2,1)S(1)}, bf16[2,128,96]{1,2,0:T(8,128)(2,1)}, pred[]{:T(512)}, bf16[2,128,96]{1,2,0:T(8,128)(2,1)}, /*i...) while((s32[]{:T(128)}, bf16[128,96]{0,1:T(8,128)(2,1)S(1)}, ...), condition=%wide.region_5.6_spmd, body=%wide.region_0.5_spmd.sunk | while | flops 395120736 | bytes 11393579 | solution.py:206
  29.3 24.6 %all_gather.15 = bf16[1024,96]{0,1:T(8,128)(2,1)S(1)} all-gather(bf16[128,96]{0,1:T(8,128)(2,1)S(1)} %bitcast_select_fusion.3), channel_id=1, replica_groups=mesh['pp'=4,'fs'=4,'tp'=2] {'tp','fs'}, dimensions={0}, use_global_device_ids=true | all-gather | bytes 221184 | tf_op jit(solution)/shard_map/while/body/eval_jaxpr/all_gather | solution.py:136
  54.1 2.3 fusion.90
  66.2 1.7 fusion.91
  67.9 1.6 rev.24
  71.7 2.2 fusion.92
  75.6 2.0 fusion.94
  77.6 1.8 copy.100
  80.2 31.0 %reduce-scatter.6.cloned.1.call-done = bf16[128,96]{1,0:T(8,128)(2,1)} async-done(((bf16[1024,96]{1,0:T(8,128)(2,1)}), bf16[128,96]{1,0:T(8,128)(2,1)}) %reduce-scatter.6.cloned.1.call-update) | async-done | bytes 24592 | tf_op jit(solution)/shard_map/while
  112.0 1.4 bitcast_dynamic-update-slice_fusion.4
  113.4 3.5 collective-permute-start
  117.0 1.5 collective-permute-done
  119.8 24.4 %all_gather.15 = bf16[1024,96]{0,1:T(8,128)(2,1)S(1)} all-gather(bf16[128,96]{0,1:T(8,128)(2,1)S(1)} %bitcast_select_fusion.3), channel_id=1, replica_groups=mesh['pp'=4,'fs'=4,'tp'=2] {'tp','fs'}, dimensions={0}, use_global_device_ids=true | all-gather | bytes 221184 | tf_op jit(solution)/shard_map/while/body/eval_jaxpr/all_gather | solution.py:136
  144.3 2.3 fusion.90
  156.4 1.7 fusion.91
  158.1 1.6 rev.24
  162.0 2.2 fusion.92
  165.8 2.0 fusion.94
  167.8 1.8 copy.100
  170.4 30.4 %reduce-scatter.6.cloned.1.call-done = bf16[128,96]{1,0:T(8,128)(2,1)} async-done(((bf16[1024,96]{1,0:T(8,128)(2,1)}), bf16[128,96]{1,0:T(8,128)(2,1)}) %reduce-scatter.6.cloned.1.call-update) | async-done | bytes 24592 | tf_op jit(solution)/shard_map/while
  201.7 1.4 bitcast_dynamic-update-slice_fusion.4
  203.1 3.3 collective-permute-start
  206.4 1.5 collective-permute-done
  209.2 24.4 %all_gather.15 = bf16[1024,96]{0,1:T(8,128)(2,1)S(1)} all-gather(bf16[128,96]{0,1:T(8,128)(2,1)S(1)} %bitcast_select_fusion.3), channel_id=1, replica_groups=mesh['pp'=4,'fs'=4,'tp'=2] {'tp','fs'}, dimensions={0}, use_global_device_ids=true | all-gather | bytes 221184 | tf_op jit(solution)/shard_map/while/body/eval_jaxpr/all_gather | solution.py:136
  233.7 2.3 fusion.90
  245.8 1.7 fusion.91
  247.5 1.6 rev.24
  251.4 2.2 fusion.92
  255.2 2.0 fusion.94
  257.2 1.8 copy.100
  259.8 30.6 %reduce-scatter.6.cloned.1.call-done = bf16[128,96]{1,0:T(8,128)(2,1)} async-done(((bf16[1024,96]{1,0:T(8,128)(2,1)}), bf16[128,96]{1,0:T(8,128)(2,1)}) %reduce-scatter.6.cloned.1.call-update) | async-done | bytes 24592 | tf_op jit(solution)/shard_map/while
  291.2 1.4 bitcast_dynamic-update-slice_fusion.4
  292.6 3.5 collective-permute-start
  296.0 1.5 collective-permute-done
  298.9 24.3 %all_gather.15 = bf16[1024,96]{0,1:T(8,128)(2,1)S(1)} all-gather(bf16[128,96]{0,1:T(8,128)(2,1)S(1)} %bitcast_select_fusion.3), channel_id=1, replica_groups=mesh['pp'=4,'fs'=4,'tp'=2] {'tp','fs'}, dimensions={0}, use_global_device_ids=true | all-gather | bytes 221184 | tf_op jit(solution)/shard_map/while/body/eval_jaxpr/all_gather | solution.py:136
  323.3 2.3 fusion.90
  335.4 1.7 fusion.91
  337.1 1.6 rev.24
  340.9 2.2 fusion.92
  344.8 2.0 fusion.94
  346.8 1.8 copy.100
  349.4 30.5 %reduce-scatter.6.cloned.1.call-done = bf16[128,96]{1,0:T(8,128)(2,1)} async-done(((bf16[1024,96]{1,0:T(8,128)(2,1)}), bf16[128,96]{1,0:T(8,128)(2,1)}) %reduce-scatter.6.cloned.1.call-update) | async-done | bytes 24592 | tf_op jit(solution)/shard_map/while
  380.8 1.4 bitcast_dynamic-update-slice_fusion.4
  382.1 3.4 collective-permute-start
  385.5 1.5 collective-permute-done
  388.4 24.3 %all_gather.15 = bf16[1024,96]{0,1:T(8,128)(2,1)S(1)} all-gather(bf16[128,96]{0,1:T(8,128)(2,1)S(1)} %bitcast_select_fusion.3), channel_id=1, replica_groups=mesh['pp'=4,'fs'=4,'tp'=2] {'tp','fs'}, dimensions={0}, use_global_device_ids=true | all-gather | bytes 221184 | tf_op jit(solution)/shard_map/while/body/eval_jaxpr/all_gather | solution.py:136
  412.8 2.3 fusion.90
  424.9 1.7 fusion.91
  426.6 1.6 rev.24
  430.5 2.2 fusion.92
  434.3 2.0 fusion.94
  436.3 1.8 copy.100
  438.9 30.6 %reduce-scatter.6.cloned.1.call-done = bf16[128,96]{1,0:T(8,128)(2,1)} async-done(((bf16[1024,96]{1,0:T(8,128)(2,1)}), bf16[128,96]{1,0:T(8,128)(2,1)}) %reduce-scatter.6.cloned.1.call-update) | async-done | bytes 24592 | tf_op jit(solution)/shard_map/while
  470.4 1.4 bitcast_dynamic-update-slice_fusion.4
  471.7 3.4 collective-permute-start
  475.2 1.5 collective-permute-done
  476.7 18.2 %psum.14 = bf16[2,128,96]{1,2,0:T(8,128)(2,1)S(1)} all-reduce(bf16[2,128,96]{1,2,0:T(8,128)(2,1)S(1)} %broadcast_select_fusion), channel_id=1, replica_groups=mesh['pp'=4,'fs'=4,'tp'=2] {'pp'}, use_global_device_ids=true, to_apply=%region_6.7 | all-reduce | flops 24576 | bytes 98304 | tf_op jit(solution)/shard_map/psum | solution.py:23
  495.0 13.7 %psum.15 = f32[2,24]{1,0:T(2,128)S(1)} all-reduce(f32[2,24]{1,0:T(2,128)S(1)} %fusion.49), channel_id=1, replica_groups=mesh['pp'=4,'fs'=4,'tp'=2] {'tp','fs'}, use_global_device_ids=true, to_apply=%region_8.9 | all-reduce | flops 48 | bytes 384 | tf_op jit(solution)/shard_map/psum | solution.py:212
  (219 shorter events, 87.6 us)
Async XLA Ops:
  9.6 4.8 copy-start.5
  9.7 6.7 %copy-start.6 = (bf16[2,24,128]{2,1,0:T(8,128)(2,1)S(1)}, bf16[2,24,128]{2,1,0:T(8,128)(2,1)}, u32[]{:S(2)}) copy-start(bf16[2,24,128]{2,1,0:T(8,128)(2,1)} %param.16) | copy-start | bytes 36868
  9.7 17.0 %copy-start.7 = (f32[1,2,4,1]{2,3,1,0:T(1,128)S(1)}, f32[1,2,4,1]{2,3,1,0:T(1,128)}, u32[]{:S(2)}) copy-start(f32[1,2,4,1]{2,3,1,0:T(1,128)} %param.24) | copy-start | bytes 100
  11.7 2.6 copy-start.4
  27.9 83.3 %reduce-scatter.6.cloned.1.call-start = ((), (), s32[]{:S(2)}) async-start(), calls=%async_computation.1 | async-start | bytes 294912 | tf_op jit(solution)/shard_map/while
  29.3 24.8 %copy-start.3 = (bf16[128,96]{0,1:T(8,128)(2,1)}, bf16[128,96]{0,1:T(8,128)(2,1)S(1)}, u32[]{:S(2)}) copy-start(bf16[128,96]{0,1:T(8,128)(2,1)S(1)} %bitcast_select_fusion.3) | copy-start | bytes 73732 | tf_op jit(solution)/shard_map/while
  56.4 0.9 copy-start
  70.9 3.1 copy-start.1
  70.9 3.1 copy-start.2
  113.4 5.1 collective-permute-start
  118.5 82.4 %reduce-scatter.6.cloned.1.call-start = ((), (), s32[]{:S(2)}) async-start(), calls=%async_computation.1 | async-start | bytes 294912 | tf_op jit(solution)/shard_map/while
  119.8 24.5 %copy-start.3 = (bf16[128,96]{0,1:T(8,128)(2,1)}, bf16[128,96]{0,1:T(8,128)(2,1)S(1)}, u32[]{:S(2)}) copy-start(bf16[128,96]{0,1:T(8,128)(2,1)S(1)} %bitcast_select_fusion.3) | copy-start | bytes 73732 | tf_op jit(solution)/shard_map/while
  146.6 0.9 copy-start
  161.1 3.1 copy-start.1
  161.1 3.1 copy-start.2
  203.1 4.8 collective-permute-start
  207.9 82.5 %reduce-scatter.6.cloned.1.call-start = ((), (), s32[]{:S(2)}) async-start(), calls=%async_computation.1 | async-start | bytes 294912 | tf_op jit(solution)/shard_map/while
  209.2 24.5 %copy-start.3 = (bf16[128,96]{0,1:T(8,128)(2,1)}, bf16[128,96]{0,1:T(8,128)(2,1)S(1)}, u32[]{:S(2)}) copy-start(bf16[128,96]{0,1:T(8,128)(2,1)S(1)} %bitcast_select_fusion.3) | copy-start | bytes 73732 | tf_op jit(solution)/shard_map/while
  236.0 0.9 copy-start
  250.5 3.1 copy-start.1
  250.5 3.1 copy-start.2
  292.6 5.0 collective-permute-start
  297.5 82.4 %reduce-scatter.6.cloned.1.call-start = ((), (), s32[]{:S(2)}) async-start(), calls=%async_computation.1 | async-start | bytes 294912 | tf_op jit(solution)/shard_map/while
  298.9 24.4 %copy-start.3 = (bf16[128,96]{0,1:T(8,128)(2,1)}, bf16[128,96]{0,1:T(8,128)(2,1)S(1)}, u32[]{:S(2)}) copy-start(bf16[128,96]{0,1:T(8,128)(2,1)S(1)} %bitcast_select_fusion.3) | copy-start | bytes 73732 | tf_op jit(solution)/shard_map/while
  325.6 0.9 copy-start
  340.1 3.1 copy-start.1
  340.1 3.1 copy-start.2
  382.1 4.9 collective-permute-start
  387.0 82.5 %reduce-scatter.6.cloned.1.call-start = ((), (), s32[]{:S(2)}) async-start(), calls=%async_computation.1 | async-start | bytes 294912 | tf_op jit(solution)/shard_map/while
  388.4 24.4 %copy-start.3 = (bf16[128,96]{0,1:T(8,128)(2,1)}, bf16[128,96]{0,1:T(8,128)(2,1)S(1)}, u32[]{:S(2)}) copy-start(bf16[128,96]{0,1:T(8,128)(2,1)S(1)} %bitcast_select_fusion.3) | copy-start | bytes 73732 | tf_op jit(solution)/shard_map/while
  415.1 0.9 copy-start
  429.6 3.1 copy-start.1
  429.6 3.1 copy-start.2
  471.7 4.9 collective-permute-start
Sparse Core Ops, SparseCore 0:
  79.5 31.6 reduce-scatter.5
  169.7 31.0 reduce-scatter.5
  259.2 31.1 reduce-scatter.5
  348.7 31.1 reduce-scatter.5
  438.2 31.2 reduce-scatter.5
where the time goes:
time: 520 us; the launch traced here: 516 us
  blocking collectives  164 us (32%)
  waiting for transfers between devices  161 us (31%)
  local copies, waits for them, and re-layouts  86.1 us (17%)
  other arithmetic  37.1 us (7%)
  matrix products  37 us (7%)
  starting transfers between devices  17.1 us (3%)
  between operations  13.2 us (3%)
    while x10, waiting for transfers between devices  153 us
    all_gather x5, blocking collectives, project(): gathered = lax.all_gather(column_block, ('tp', 'fs'), axis=0, tiled=True)  122 us
    mul x30, local copies, waits for them, and re-layouts, centred_conv(): running = running + padded[offset:offset + length] * conv_taps[offset]  20.8 us
    psum x1, blocking collectives, spread(): return lax.psum(kept, axis)  18.2 us
    rev x20, local copies, waits for them, and re-layouts, duality_mix(): bwd_cum = jnp.flip(jnp.cumsum(jnp.flip(log_decay[:, 1], 0), axis=0), 0)  17.8 us
    ppermute x5, starting transfers between devices, from_behind(): return lax.ppermute(block, axis, route)  17.1 us
    psum x1, blocking collectives, body(): total_squares = lax.psum(partial_squares, ('tp', 'fs'))  13.7 us
    while x50, local copies, waits for them, and re-layouts  13.1 us
  transfers between devices with their start and end apart: 10, of which 10 were waited for; matrix products, arithmetic and copies ran while one was open for 1% of the time, Pallas kernels for 0%

commit v1 on v0

--- a/solution.py
+++ b/solution.py
@@ -1,6 +1,10 @@
+import functools
+
 import jax
 import jax.numpy as jnp
 from jax import lax
+from jax.experimental import pallas as pl
+from jax.experimental.pallas import tpu as pltpu
 from jax.sharding import PartitionSpec as P
 
 epsilon = 1e-06
@@ -215,9 +219,511 @@
     return jnp.swapaxes(result, 1, 2)
 
 
+MESH = pl.DeviceIdType.MESH
+NT_DIMS = (((1,), (1,)), ((), ()))
+NN_DIMS = (((1,), (0,)), ((), ()))
+
+
+def silu(x):
+    return 0.5 * x * (1.0 + jnp.tanh(0.5 * x))
+
+
+def matmul(left, right, dims=NN_DIMS, precision=None):
+    return lax.dot_general(
+        left, right, dims, precision=precision, preferred_element_type=jnp.float32
+    )
+
+
+def relay_kernel(
+    sizes,
+    in_ref,
+    gain_ref,
+    gate_w,
+    value_w,
+    write_w,
+    read_w,
+    step_w,
+    bias_ref,
+    decay_ref,
+    skip_ref,
+    tap_v,
+    tap_w,
+    tap_r,
+    out_w,
+    out_ref,
+    entry,
+    acts,
+    partial,
+    arrived,
+    produced,
+    leaving,
+    final_in,
+    squares,
+    square_in,
+    column,
+    padded,
+    sem_entry_s,
+    sem_entry_r,
+    sem_rs_s,
+    sem_rs_r,
+    sem_hop_s,
+    sem_ag_r,
+    sem_twin_s,
+    sem_fin_s,
+    sem_fin_r,
+    sem_sq_s,
+    sem_sq_r,
+    sem_local,
+):
+    sections, ring, cores = sizes["pp"], sizes["fs"], sizes["tp"]
+    owners = ring * cores
+    micro, share, block = in_ref.shape
+    length = share * sections
+    width = owners * block
+    inner = gate_w.shape[0]
+    groups, state = tap_w.shape[1], tap_w.shape[2]
+    taps, heads, head = tap_v.shape
+    per_group = heads // groups
+    half = taps // 2
+    s = lax.axis_index("pp")
+    z = lax.axis_index("fs")
+    c = lax.axis_index("tp")
+    j = c * ring + z
+    last = sections - 1
+    me = s * owners + j
+
+    def place(section, owner):
+        return {"pp": section, "fs": lax.rem(owner, ring), "tp": owner // ring}
+
+    barrier = pltpu.get_barrier_semaphore()
+    for step in range(1, sections * owners):
+        other = lax.rem(me + step, sections * owners)
+        pl.semaphore_signal(
+            barrier,
+            inc=1,
+            device_id=place(other // owners, lax.rem(other, owners)),
+            device_id_type=MESH,
+        )
+    pl.semaphore_wait(barrier, sections * owners - 1)
+
+    def remote(src, dst, send_sem, recv_sem, target):
+        return pltpu.make_async_remote_copy(
+            src_ref=src,
+            dst_ref=dst,
+            send_sem=send_sem,
+            recv_sem=recv_sem,
+            device_id=target,
+            device_id_type=MESH,
+        )
+
+    def entry_copy(m, step):
+        owner = lax.rem(j + step, owners)
+        return remote(
+            in_ref.at[m],
+            entry.at[m, j, s],
+            sem_entry_s.at[m, step],
+            sem_entry_r.at[m, j, s],
+            place(0, owner),
+        )
+
+    def entry_own(m):
+        return pltpu.make_async_copy(in_ref.at[m], entry.at[m, j, s], sem_entry_r.at[m, j, s])
+
+    for m in range(micro):
+        for step in range(1, owners):
+            entry_copy(m, step).start()
+
+        @pl.when(s == 0)
+        def _():
+            entry_own(m).start()
+
+        @pl.when(s != 0)
+        def _():
+            entry_copy(m, 0).start()
+
+    lane_v = lax.broadcasted_iota(jnp.int32, (1, heads * head), 1)
+    row8 = lax.broadcasted_iota(jnp.int32, (2 * heads, 1), 0)
+    bias_col = jnp.zeros((2 * heads, 1), jnp.float32)
+    decay_col = jnp.zeros((2 * heads, 1), jnp.float32)
+    skip_row = jnp.zeros((1, heads * head), jnp.float32)
+    for i in range(2 * heads):
+        d, h = i // heads, i % heads
+        bias_col = jnp.where(row8 == i, bias_ref[d, h], bias_col)
+        decay_col = jnp.where(row8 == i, decay_ref[d, h], decay_col)
+    for h in range(heads):
+        skip_row = jnp.where(lane_v // head == h, skip_ref[h], skip_row)
+    decay_col = -jnp.exp(decay_col)
+    value_taps = [
+        jnp.concatenate([tap_v[k, h : h + 1, :] for h in range(heads)], axis=1)
+        for k in range(taps)
+    ]
+    tpos = lax.broadcasted_iota(jnp.int32, (length, length), 0)
+    spos = lax.broadcasted_iota(jnp.int32, (length, length), 1)
+    lower = spos <= tpos
+    diag = spos == tpos
+    tri_low = jnp.where(lower, 1.0, 0.0)
+    tri_up = jnp.where(spos >= tpos, 1.0, 0.0)
+    edge = jnp.zeros((8, 128), jnp.float32)
+    for q in range(padded.shape[0]):
+        padded[q, 0:8, :] = edge
+        padded[q, 8 + length : 16 + length, :] = edge
+
+    def conv_act(slot, signal, rows):
+        padded[slot, 8 : 8 + length, :] = signal.astype(jnp.bfloat16).astype(jnp.float32)
+        start = 8 - half
+        total = padded[slot, start : start + length, :] * rows[0]
+        for k in range(1, taps):
+            total = total + padded[slot, start + k : start + k + length, :] * rows[k]
+        return silu(total).astype(jnp.bfloat16)
+
+    def twin_copy(m, zz, step):
+        slot = c * ring + zz
+        other = lax.rem(c + step, cores)
+        return remote(
+            acts.at[m, slot],
+            acts.at[m, slot],
+            sem_twin_s.at[m, zz, step - 1],
+            sem_ag_r.at[m, slot],
+            {"pp": s, "fs": z, "tp": other},
+        )
+
+    def wait_block(m, slot):
+        remote(
+            acts.at[m, slot],
+            acts.at[m, slot],
+            sem_twin_s.at[m, 0, 0],
+            sem_ag_r.at[m, slot],
+            place(s, slot),
+        ).wait_recv()
+
+    def receive(m):
+        @pl.when(s == 0)
+        def _():
+            for k in range(owners):
+                for p in range(sections):
+                    pltpu.make_async_copy(
+                        in_ref.at[m], entry.at[m, k, p], sem_entry_r.at[m, k, p]
+                    ).wait()
+            for k in range(owners):
+                acts[m, k] = jnp.concatenate(
+                    [entry[m, k, p].astype(jnp.float32) for p in range(sections)], axis=0
+                ).astype(jnp.bfloat16)
+
+        @pl.when(s != 0)
+        def _():
+            for zz in range(ring):
+                wait_block(m, c * ring + zz)
+                for step in range(1, cores):
+                    twin_copy(m, zz, step).start()
+            for step in range(1, cores):
+                other = lax.rem(c + step, cores)
+                for zz in range(ring):
+                    wait_block(m, other * ring + zz)
+
+    def rs_copy(m, step):
+        owner = lax.rem(j + step, owners)
+        return remote(
+            partial.at[m, owner],
+            arrived.at[m, j],
+            sem_rs_s.at[m, step - 1],
+            sem_rs_r.at[m, j],
+            place(s, owner),
+        )
+
+    def mix(m):
+        x = [acts[m, k].astype(jnp.float32) for k in range(owners)]
+        total = x[0] * x[0]
+        for k in range(1, owners):
+            total = total + x[k] * x[k]
+        scale = lax.rsqrt(jnp.sum(total, axis=1, keepdims=True) / width + epsilon)
+        normed = jnp.concatenate(
+            [
+                (x[k] * scale * gain_ref[:, k * block : (k + 1) * block]).astype(jnp.bfloat16)
+                for k in range(owners)
+            ],
+            axis=1,
+        )
+        step_row = matmul(step_w[...], normed, NT_DIMS) + bias_col
+        dt = jnp.maximum(step_row, 0.0) + jnp.log1p(jnp.exp(-jnp.abs(step_row)))
+        a = dt * decay_col
+        high = lax.Precision.HIGHEST
+        fwd_row = matmul(a, tri_low, NT_DIMS, high)
+        bwd_row = matmul(a, tri_up, NT_DIMS, high)
+        fwd_col = matmul(tri_low, a, NT_DIMS, high)
+        bwd_col = matmul(tri_up, a, NT_DIMS, high)
+        value_raw = matmul(normed, value_w[...], NT_DIMS)
+        write_raw = matmul(normed, write_w[...])
+        read_raw = matmul(normed, read_w[...])
+        gate_raw = matmul(normed, gate_w[...], NT_DIMS)
+        pieces = inner // 128
+        value = jnp.concatenate(
+            [
+                conv_act(
+                    i,
+                    value_raw[:, i * 128 : (i + 1) * 128],
+                    [value_taps[k][:, i * 128 : (i + 1) * 128] for k in range(taps)],
+                )
+                for i in range(pieces)
+            ],
+            axis=1,
+        )
+        y = jnp.zeros((length, inner), jnp.float32)
+        for g in range(groups):
+            write = conv_act(
+                pieces + 2 * g,
+                write_raw[:, g * state : (g + 1) * state],
+                [tap_w[k, g : g + 1, :] for k in range(taps)],
+            )
+            read = conv_act(
+                pieces + 2 * g + 1,
+                read_raw[:, g * state : (g + 1) * state],
+                [tap_r[k, g : g + 1, :] for k in range(taps)],
+            )
+            scores = matmul(read, write, NT_DIMS)
+            for e in range(per_group):
+                h = g * per_group + e
+                b = heads + h
+                fwd_gap = fwd_col[:, h : h + 1] - fwd_row[h : h + 1, :]
+                bwd_gap = bwd_col[:, b : b + 1] - bwd_row[b : b + 1, :]
+                dt_f, dt_b = dt[h : h + 1, :], dt[b : b + 1, :]
+                weight = jnp.exp(jnp.where(lower, fwd_gap, bwd_gap)) * jnp.where(
+                    lower, dt_f, dt_b
+                ) + jnp.where(diag, dt_b, 0.0)
+                mixed = matmul((scores * weight).astype(jnp.bfloat16), value)
+                y = jnp.where(lane_v // head == h, mixed, y)
+        y = y + skip_row * value.astype(jnp.float32)
+        gate = gate_raw.astype(jnp.bfloat16).astype(jnp.float32)
+        gated = (y * silu(gate)).astype(jnp.bfloat16)
+        sums = matmul(gated, out_w[...])
+        for k in range(owners):
+            partial[m, k] = sums[:, k * block : (k + 1) * block].astype(jnp.bfloat16)
+        for step in range(1, owners):
+            rs_copy(m, step).start()
+
+    def hop_copy(m, zz):
+        return remote(
+            produced.at[m],
+            acts.at[m, j],
+            sem_hop_s.at[m, zz],
+            sem_ag_r.at[m, j],
+            {"pp": lax.rem(s + 1, sections), "fs": zz, "tp": c},
+        )
+
+    def fin_copy(m, p):
+        return remote(
+            leaving.at[m, p],
+            final_in.at[m],
+            sem_fin_s.at[m, p],
+            sem_fin_r.at[m],
+            {"pp": p, "fs": z, "tp": c},
+        )
+
+    def sq_copy(m, step):
+        other = lax.rem(me + step, sections * owners)
+        return remote(
+            squares.at[m],
+            square_in.at[m, j],
+            sem_sq_s.at[m, step - 1],
+            sem_sq_r.at[m, j],
+            place(other // owners, lax.rem(other, owners)),
+        )
+
+    def reduce(m):
+        total = partial[m, j].astype(jnp.float32)
+        for step in range(1, owners):
+            source = lax.rem(j + step, owners)
+            remote(
+                partial.at[m, source],
+                arrived.at[m, source],
+                sem_rs_s.at[m, 0],
+                sem_rs_r.at[m, source],
+                place(s, source),
+            ).wait_recv()
+            total = total + arrived[m, source].astype(jnp.float32)
+        branch = total.astype(jnp.bfloat16).astype(jnp.float32)
+        made = (acts[m, j].astype(jnp.float32) + 0.5 * branch).astype(jnp.bfloat16)
+
+        @pl.when(s != last)
+        def _():
+            produced[m] = made
+            for zz in range(ring):
+                hop_copy(m, zz).start()
+
+        @pl.when(s == last)
+        def _():
+            o = made.astype(jnp.float32)
+            for p in range(sections):
+                leaving[m, p] = o[p * share : (p + 1) * share].astype(jnp.bfloat16)
+            col = jnp.sum(o * o, axis=1, keepdims=True)
+            full = jnp.concatenate(
+                [
+                    jnp.broadcast_to(col, (length, 128)),
+                    jnp.zeros((128 - length, 128), jnp.float32),
+                ],
+                axis=0,
+            )
+            row = jnp.transpose(full)[0:8, :]
+            squares[m] = row
+            square_in[m, j] = row
+            for p in range(last):
+                fin_copy(m, p).start()
+            for step in range(1, sections * owners):
+                sq_copy(m, step).start()
+            pltpu.make_async_copy(leaving.at[m, last], final_in.at[m], sem_local.at[m]).start()
+
+    def finish(m):
+        @pl.when(s != last)
+        def _():
+            fin_copy(m, 0).wait_recv()
+
+        @pl.when(s == last)
+        def _():
+            pltpu.make_async_copy(leaving.at[m, last], final_in.at[m], sem_local.at[m]).wait()
+
+        for k in range(owners):
+
+            @pl.when((s != last) | (j != k))
+            def _():
+                remote(
+                    squares.at[m],
+                    square_in.at[m, k],
+                    sem_sq_s.at[m, 0],
+                    sem_sq_r.at[m, k],
+                    place(last, k),
+                ).wait_recv()
+
+        total = square_in[m, 0]
+        for k in range(1, owners):
+            total = total + square_in[m, k]
+        scale = lax.rsqrt(total / width + epsilon)
+        column[m] = jnp.transpose(jnp.broadcast_to(scale[0:1, :], (128, 128)))
+        own = column[m, pl.ds(pl.multiple_of(s * share, 8), share), :]
+        out_ref[m] = (final_in[m].astype(jnp.float32) * own).astype(jnp.bfloat16)
+
+    for m in range(micro):
+        receive(m)
+        mix(m)
+    for m in range(micro):
+        reduce(m)
+    for m in range(micro):
+        finish(m)
+
+    for m in range(micro):
+        for step in range(1, owners):
+            entry_copy(m, step).wait_send()
+            rs_copy(m, step).wait_send()
+
+        @pl.when(s != 0)
+        def _():
+            entry_copy(m, 0).wait_send()
+            for zz in range(ring):
+                for step in range(1, cores):
+                    twin_copy(m, zz, step).wait_send()
+
+        @pl.when(s != last)
+        def _():
+            for zz in range(ring):
+                hop_copy(m, zz).wait_send()
+
+        @pl.when(s == last)
+        def _():
+            for p in range(last):
+                fin_copy(m, p).wait_send()
+            for step in range(1, sections * owners):
+                sq_copy(m, step).wait_send()
+
+
+def fused_body(
+    micro_in,
+    norm_gain,
+    proj_gate,
+    proj_value,
+    proj_write,
+    proj_read,
+    proj_step,
+    step_bias,
+    decay_log,
+    skip_gain,
+    conv_value,
+    conv_write,
+    conv_read,
+    proj_out,
+    sizes,
+):
+    sections, ring, cores = sizes["pp"], sizes["fs"], sizes["tp"]
+    owners = ring * cores
+    micro, share, block = micro_in.shape
+    length = share * sections
+    width = norm_gain.shape[1]
+    taps = conv_value.shape[1]
+    head = conv_value.shape[4]
+    heads = conv_value.shape[2] * conv_value.shape[3]
+    groups, state = conv_write.shape[2:]
+    inner = heads * head
+    args = (
+        micro_in,
+        norm_gain,
+        jnp.transpose(proj_gate[0], (1, 2, 3, 0)).reshape(inner, width),
+        jnp.transpose(proj_value[0], (1, 2, 3, 0)).reshape(inner, width),
+        proj_write[0].reshape(width, groups * state),
+        proj_read[0].reshape(width, groups * state),
+        jnp.transpose(proj_step[0], (1, 2, 3, 0)).reshape(2 * heads, width),
+        step_bias[0].reshape(2, heads),
+        decay_log[0].reshape(2, heads),
+        skip_gain[0].reshape(heads),
+        conv_value[0].reshape(taps, heads, head),
+        conv_write[0],
+        conv_read[0],
+        proj_out[0].reshape(inner, width),
+    )
+    vmem = pl.BlockSpec(memory_space=pltpu.VMEM)
+    smem = pl.BlockSpec(memory_space=pltpu.SMEM)
+    bf16, f32 = jnp.bfloat16, jnp.float32
+    dma = pltpu.SemaphoreType.DMA
+    pads = inner // 128 + 2 * groups
+    return pl.pallas_call(
+        functools.partial(relay_kernel, sizes),
+        out_shape=jax.ShapeDtypeStruct(micro_in.shape, bf16),
+        in_specs=[vmem] * 7 + [smem] * 3 + [vmem] * 4,
+        out_specs=vmem,
+        scratch_shapes=[
+            pltpu.VMEM((micro, owners, sections, share, block), bf16),
+            pltpu.VMEM((micro, owners, length, block), bf16),
+            pltpu.VMEM((micro, owners, length, block), bf16),
+            pltpu.VMEM((micro, owners, length, block), bf16),
+            pltpu.VMEM((micro, length, block), bf16),
+            pltpu.VMEM((micro, sections, share, block), bf16),
+            pltpu.VMEM((micro, share, block), bf16),
+            pltpu.VMEM((micro, 8, 128), f32),
+            pltpu.VMEM((micro, owners, 8, 128), f32),
+            pltpu.VMEM((micro, 128, 128), f32),
+            pltpu.VMEM((pads, length + 16, 128), f32),
+            dma((micro, owners)),
+            dma((micro, owners, sections)),
+            dma((micro, owners - 1)),
+            dma((micro, owners)),
+            dma((micro, ring)),
+            dma((micro, owners)),
+            dma((micro, ring, cores - 1)),
+            dma((micro, sections)),
+            dma((micro,)),
+            dma((micro, sections * owners - 1)),
+            dma((micro, owners)),
+            dma((micro,)),
+        ],
+        compiler_params=pltpu.CompilerParams(collective_id=0, has_side_effects=True),
+    )(*args)
+
+
 def solution(mesh):
+    sizes = dict(mesh.shape)
+
+    def chosen(micro_in, *weights):
+        fits = micro_in.shape[2] % 128 == 0 and micro_in.shape[1] % 8 == 0
+        return (fused_body if fits else body)(micro_in, *weights, *(() if not fits else (sizes,)))
+
     return jax.shard_map(
-        body,
+        chosen,
         mesh=mesh,
         in_specs=(
             P(None, "pp", ("tp", "fs")),

time: 520 us -> 89.6 us (0.17)
  blocking collectives: 164 us -> 0 us
  waiting for transfers between devices: 161 us -> 0 us
  Pallas kernels: 0 us -> 83.4 us
  local copies, waits for them, and re-layouts: 86.1 us -> 5.86 us
  other arithmetic: 37.1 us -> 0 us
  matrix products: 37 us -> 0 us
  starting transfers between devices: 17.1 us -> 0 us
  between operations: 13.2 us -> 0.01 us
    while x10 -> x0, waiting for transfers between devices: 153 us -> none
    all_gather x6 -> x0, blocking collectives: 132 us -> none  [the longest x5 122 us: project(): gathered = lax.all_gather(column_block, ('tp', 'fs'), axis=0, tiled=True)]
    pallas_call x0 -> x1, Pallas kernels: none -> 83.4 us  [fused_body(): pl.pallas_call(functools.partial(relay_kernel, sizes), out_shape=jax.Shap...]
    dot_general x20 -> x0, matrix products: 37 us -> none  [the longest x5 11.3 us: project(): lax.dot_general(normed, weight_all, (((0,), (0,)), ((), ())), preferred_e...]
    psum x2 -> x0, blocking collectives: 31.9 us -> none  [the longest x1 18.2 us: spread(): return lax.psum(kept, axis)]
    mul x35 -> x0, local copies, waits for them, and re-layouts: 20.8 us -> none  [the longest x30 20.8 us: centred_conv(): running = running + padded[offset:offset + length] * conv_taps[offset]]
    rev x20 -> x0, local copies, waits for them, and re-layouts: 17.8 us -> none  [duality_mix(): bwd_cum = jnp.flip(jnp.cumsum(jnp.flip(log_decay[:, 1], 0), axis=0), 0)]
    ppermute x5 -> x0, starting transfers between devices: 17.1 us -> none  [from_behind(): return lax.ppermute(block, axis, route)]
  transfers between devices with their start and end apart: 10 -> 0, of which waited for: 10 -> 0; matrix products, arithmetic and copies ran while one was open for 1% -> 0% of each run, Pallas kernels for 0% -> 0%
where the time goes in v1:
time: 89.6 us; the launch traced here: 89.2 us
  Pallas kernels  83.4 us (93%)
  local copies, waits for them, and re-layouts  5.86 us (7%)
    pallas_call x1, Pallas kernels, fused_body(): pl.pallas_call(functools.partial(relay_kernel, sizes), out_shape=jax.Shap...  83.4 us
    another operation x1, local copies, waits for them, and re-layouts, fused_body(): proj_read[0].reshape(width, groups * state)  3.22 us
    unnamed x3, local copies, waits for them, and re-layouts  2.03 us

profile of v1, /device:TPU:0, one launch (start us, length us, event | category | flops | bytes accessed | tf_op | source)
XLA Modules:
  0.0 89.2 jit_solution(7511239405922317329)
XLA Ops:
  0.0 0.0 copy-start
  0.0 0.7 copy-done
  0.7 0.6 reshape.11.step_w
  1.3 3.2 %copy_bitcast_fusion = (bf16[1024,512]{1,0:T(8,128)(2,1)}, bf16[1024,512]{1,0:T(8,128)(2,1)}) fusion(bf16[128,8,4,128]{3,2,1,0:T(4,128)(2,1)} %bitcast.30, bf16[128,8,4,128]{3,2,1,0:T(4,128)(2,1)} %bitcast.31), kind=kLoop, calls=%fused_computation | loop fusion | bytes 4194304 | tf_op jit(solution)/shard_map/reshape;squeeze | solution.py:669
  4.6 83.4 %shard_map.136 = bf16[2,24,128]{2,1,0:T(8,128)(2,1)} custom-call(bf16[2,24,128]{2,1,0:T(8,128)(2,1)} %in_ref.1, f32[1,1024]{1,0:T(1,128)} %gain_ref.1, bf16[256,1024]{1,0:T(8,128)(2,1)} %bitcast.32, bf16[256,1024]{1,0:T(8,128)(2,1)} %bitcast.33, bf16[1024,512]{1,0:T(8,128)(2,1)} %get-tuple-element.6.write_w, bf16[1024,512]{1,0:T(8,128)(2,1)} %get-tuple-element.5.read_w, ...), custom_call_target="tpu_custom_call" | custom-call | tf_op jit(solution)/shard_map/pallas_call | solution.py:684
  87.9 1.3 %copy.20 = bf16[2,24,128]{2,1,0:T(8,128)(2,1)} copy(bf16[2,24,128]{2,1,0:T(8,128)(2,1)} %shard_map.136) | data formatting | bytes 24576
Async XLA Ops:
  0.0 0.7 copy-start

commit v2 on v1

--- a/solution.py
+++ b/solution.py
@@ -238,10 +238,10 @@
     sizes,
     in_ref,
     gain_ref,
-    gate_w,
-    value_w,
-    write_w,
-    read_w,
+    gate_hbm,
+    value_hbm,
+    write_hbm,
+    read_hbm,
     step_w,
     bias_ref,
     decay_ref,
@@ -249,11 +249,19 @@
     tap_v,
     tap_w,
     tap_r,
+    out_hbm,
+    out_ref,
+    gate_w,
+    value_w,
+    raw_w,
+    mixed_w,
     out_w,
-    out_ref,
     entry,
     acts,
     partial,
+    from_twin,
+    own_sum,
+    pair_sum,
     arrived,
     produced,
     leaving,
@@ -262,8 +270,11 @@
     square_in,
     column,
     padded,
+    sem_load,
     sem_entry_s,
     sem_entry_r,
+    sem_pre_s,
+    sem_pre_r,
     sem_rs_s,
     sem_rs_r,
     sem_hop_s,
@@ -295,6 +306,22 @@
     def place(section, owner):
         return {"pp": section, "fs": lax.rem(owner, ring), "tp": owner // ring}
 
+    loads = [
+        pltpu.make_async_copy(src, dst, sem_load.at[i])
+        for i, (src, dst) in enumerate(
+            (
+                (write_hbm, raw_w.at[0]),
+                (read_hbm, raw_w.at[1]),
+                (value_hbm, value_w),
+                (gate_hbm, gate_w),
+                (out_hbm, out_w),
+            )
+        )
+    ]
+    for load in loads:
+        load.start()
+    far_first = sorted(range(1, ring), key=lambda k: -min(k, ring - k))
+
     barrier = pltpu.get_barrier_semaphore()
     for step in range(1, sections * owners):
         other = lax.rem(me + step, sections * owners)
@@ -317,20 +344,19 @@
         )
 
     def entry_copy(m, step):
-        owner = lax.rem(j + step, owners)
         return remote(
             in_ref.at[m],
-            entry.at[m, j, s],
+            entry.at[m, z, s],
             sem_entry_s.at[m, step],
-            sem_entry_r.at[m, j, s],
-            place(0, owner),
+            sem_entry_r.at[m, z, s],
+            {"pp": 0, "fs": lax.rem(z + step, ring), "tp": c},
         )
 
     def entry_own(m):
-        return pltpu.make_async_copy(in_ref.at[m], entry.at[m, j, s], sem_entry_r.at[m, j, s])
+        return pltpu.make_async_copy(in_ref.at[m], entry.at[m, z, s], sem_entry_r.at[m, z, s])
 
     for m in range(micro):
-        for step in range(1, owners):
+        for step in far_first:
             entry_copy(m, step).start()
 
         @pl.when(s == 0)
@@ -368,6 +394,25 @@
         padded[q, 0:8, :] = edge
         padded[q, 8 + length : 16 + length, :] = edge
 
+    for load in loads:
+        load.wait()
+    chunk = 256
+    rows_per = chunk // groups
+    to_row = lax.broadcasted_iota(jnp.int32, (chunk, chunk), 0)
+    from_row = lax.broadcasted_iota(jnp.int32, (chunk, chunk), 1)
+    order = jnp.where(
+        from_row == lax.rem(to_row, rows_per) * groups + to_row // rows_per, 1.0, 0.0
+    ).astype(jnp.bfloat16)
+    for i in range(2):
+        for b in range(width // rows_per):
+            sorted_rows = matmul(order, raw_w[i, b * chunk : (b + 1) * chunk, :]).astype(
+                jnp.bfloat16
+            )
+            for g in range(groups):
+                mixed_w[
+                    i, b * rows_per : (b + 1) * rows_per, g * state : (g + 1) * state
+                ] = sorted_rows[g * rows_per : (g + 1) * rows_per]
+
     def conv_act(slot, signal, rows):
         padded[slot, 8 : 8 + length, :] = signal.astype(jnp.bfloat16).astype(jnp.float32)
         start = 8 - half
@@ -397,37 +442,49 @@
         ).wait_recv()
 
     def receive(m):
-        @pl.when(s == 0)
-        def _():
-            for k in range(owners):
+        for step in range(ring):
+            zz = lax.rem(z + step, ring)
+            slot = c * ring + zz
+
+            @pl.when(s == 0)
+            def _():
                 for p in range(sections):
                     pltpu.make_async_copy(
-                        in_ref.at[m], entry.at[m, k, p], sem_entry_r.at[m, k, p]
+                        in_ref.at[m], entry.at[m, zz, p], sem_entry_r.at[m, zz, p]
                     ).wait()
-            for k in range(owners):
-                acts[m, k] = jnp.concatenate(
-                    [entry[m, k, p].astype(jnp.float32) for p in range(sections)], axis=0
+                acts[m, slot] = jnp.concatenate(
+                    [entry[m, zz, p].astype(jnp.float32) for p in range(sections)], axis=0
                 ).astype(jnp.bfloat16)
 
-        @pl.when(s != 0)
-        def _():
-            for zz in range(ring):
-                wait_block(m, c * ring + zz)
-                for step in range(1, cores):
-                    twin_copy(m, zz, step).start()
-            for step in range(1, cores):
-                other = lax.rem(c + step, cores)
-                for zz in range(ring):
-                    wait_block(m, other * ring + zz)
+            @pl.when(s != 0)
+            def _():
+                wait_block(m, slot)
+
+            for twin in range(1, cores):
+                twin_copy(m, zz, twin).start()
+        for twin in range(1, cores):
+            other = lax.rem(c + twin, cores)
+            for step in range(ring):
+                wait_block(m, other * ring + lax.rem(z + step, ring))
+
+    def pre_copy(m, twin, zz):
+        other = lax.rem(c + twin, cores)
+        return remote(
+            partial.at[m, twin - 1, zz],
+            from_twin.at[m, twin - 1, zz],
+            sem_pre_s.at[m, twin - 1, zz],
+            sem_pre_r.at[m, twin - 1, zz],
+            {"pp": s, "fs": z, "tp": other},
+        )
 
     def rs_copy(m, step):
-        owner = lax.rem(j + step, owners)
+        zz = lax.rem(z + step, ring)
         return remote(
-            partial.at[m, owner],
-            arrived.at[m, j],
+            pair_sum.at[m, zz],
+            arrived.at[m, z],
             sem_rs_s.at[m, step - 1],
-            sem_rs_r.at[m, j],
-            place(s, owner),
+            sem_rs_r.at[m, z],
+            {"pp": s, "fs": zz, "tp": c},
         )
 
     def mix(m):
@@ -443,7 +500,10 @@
             ],
             axis=1,
         )
-        step_row = matmul(step_w[...], normed, NT_DIMS) + bias_col
+        step_row = (
+            jnp.concatenate([matmul(step_w[d], normed, NT_DIMS) for d in range(2)], axis=0)
+            + bias_col
+        )
         dt = jnp.maximum(step_row, 0.0) + jnp.log1p(jnp.exp(-jnp.abs(step_row)))
         a = dt * decay_col
         high = lax.Precision.HIGHEST
@@ -452,8 +512,8 @@
         fwd_col = matmul(tri_low, a, NT_DIMS, high)
         bwd_col = matmul(tri_up, a, NT_DIMS, high)
         value_raw = matmul(normed, value_w[...], NT_DIMS)
-        write_raw = matmul(normed, write_w[...])
-        read_raw = matmul(normed, read_w[...])
+        write_raw = matmul(normed, mixed_w[0])
+        read_raw = matmul(normed, mixed_w[1])
         gate_raw = matmul(normed, gate_w[...], NT_DIMS)
         pieces = inner // 128
         value = jnp.concatenate(
@@ -494,19 +554,44 @@
         y = y + skip_row * value.astype(jnp.float32)
         gate = gate_raw.astype(jnp.bfloat16).astype(jnp.float32)
         gated = (y * silu(gate)).astype(jnp.bfloat16)
-        sums = matmul(gated, out_w[...])
-        for k in range(owners):
-            partial[m, k] = sums[:, k * block : (k + 1) * block].astype(jnp.bfloat16)
-        for step in range(1, owners):
+        span = ring * block
+
+        def half_sums(core):
+            start = pl.multiple_of(core * span, 128)
+            return matmul(gated, out_w[:, pl.ds(start, span)])
+
+        for twin in range(1, cores):
+            sums = half_sums(lax.rem(c + twin, cores))
+            for zz in range(ring):
+                partial[m, twin - 1, zz] = sums[:, zz * block : (zz + 1) * block].astype(
+                    jnp.bfloat16
+                )
+                pre_copy(m, twin, zz).start()
+        sums = half_sums(c)
+        for zz in range(ring):
+            own_sum[m, zz] = sums[:, zz * block : (zz + 1) * block]
+
+    def pair(m, zz):
+        total = own_sum[m, zz]
+        for twin in range(1, cores):
+            pre_copy(m, twin, zz).wait_recv()
+            total = total + from_twin[m, twin - 1, zz].astype(jnp.float32)
+        return total
+
+    def send_pairs(m):
+        for step in far_first:
+            zz = lax.rem(z + step, ring)
+            pair_sum[m, zz] = pair(m, zz).astype(jnp.bfloat16)
             rs_copy(m, step).start()
-
-    def hop_copy(m, zz):
+        own_sum[m, z] = pair(m, z)
+
+    def hop_copy(m, step):
         return remote(
             produced.at[m],
             acts.at[m, j],
-            sem_hop_s.at[m, zz],
+            sem_hop_s.at[m, step],
             sem_ag_r.at[m, j],
-            {"pp": lax.rem(s + 1, sections), "fs": zz, "tp": c},
+            {"pp": lax.rem(s + 1, sections), "fs": lax.rem(z + step, ring), "tp": c},
         )
 
     def fin_copy(m, p):
@@ -529,15 +614,15 @@
         )
 
     def reduce(m):
-        total = partial[m, j].astype(jnp.float32)
-        for step in range(1, owners):
-            source = lax.rem(j + step, owners)
+        total = own_sum[m, z]
+        for step in range(1, ring):
+            source = lax.rem(z + step, ring)
             remote(
-                partial.at[m, source],
+                pair_sum.at[m, source],
                 arrived.at[m, source],
-                sem_rs_s.at[m, 0],
+                sem_rs_s.at[m, step - 1],
                 sem_rs_r.at[m, source],
-                place(s, source),
+                {"pp": s, "fs": source, "tp": c},
             ).wait_recv()
             total = total + arrived[m, source].astype(jnp.float32)
         branch = total.astype(jnp.bfloat16).astype(jnp.float32)
@@ -546,8 +631,8 @@
         @pl.when(s != last)
         def _():
             produced[m] = made
-            for zz in range(ring):
-                hop_copy(m, zz).start()
+            for step in (*far_first, 0):
+                hop_copy(m, step).start()
 
         @pl.when(s == last)
         def _():
@@ -562,7 +647,7 @@
                 ],
                 axis=0,
             )
-            row = jnp.transpose(full)[0:8, :]
+            row = jnp.transpose(full)[0:1, :]
             squares[m] = row
             square_in[m, j] = row
             for p in range(last):
@@ -596,29 +681,31 @@
         for k in range(1, owners):
             total = total + square_in[m, k]
         scale = lax.rsqrt(total / width + epsilon)
-        column[m] = jnp.transpose(jnp.broadcast_to(scale[0:1, :], (128, 128)))
+        column[m] = jnp.transpose(jnp.broadcast_to(scale, (128, 128)))
         own = column[m, pl.ds(pl.multiple_of(s * share, 8), share), :]
         out_ref[m] = (final_in[m].astype(jnp.float32) * own).astype(jnp.bfloat16)
 
     for m in range(micro):
         receive(m)
         mix(m)
+        send_pairs(m)
     for m in range(micro):
         reduce(m)
     for m in range(micro):
         finish(m)
 
     for m in range(micro):
-        for step in range(1, owners):
+        for step in range(1, ring):
             entry_copy(m, step).wait_send()
             rs_copy(m, step).wait_send()
+        for twin in range(1, cores):
+            for zz in range(ring):
+                pre_copy(m, twin, zz).wait_send()
+                twin_copy(m, zz, twin).wait_send()
 
         @pl.when(s != 0)
         def _():
             entry_copy(m, 0).wait_send()
-            for zz in range(ring):
-                for step in range(1, cores):
-                    twin_copy(m, zz, step).wait_send()
 
         @pl.when(s != last)
         def _():
@@ -665,9 +752,9 @@
         norm_gain,
         jnp.transpose(proj_gate[0], (1, 2, 3, 0)).reshape(inner, width),
         jnp.transpose(proj_value[0], (1, 2, 3, 0)).reshape(inner, width),
-        proj_write[0].reshape(width, groups * state),
-        proj_read[0].reshape(width, groups * state),
-        jnp.transpose(proj_step[0], (1, 2, 3, 0)).reshape(2 * heads, width),
+        proj_write[0].reshape(width * groups, state),
+        proj_read[0].reshape(width * groups, state),
+        jnp.transpose(proj_step[0], (1, 2, 3, 0)).reshape(2, heads, width),
         step_bias[0].reshape(2, heads),
         decay_log[0].reshape(2, heads),
         skip_gain[0].reshape(heads),
@@ -678,30 +765,42 @@
     )
     vmem = pl.BlockSpec(memory_space=pltpu.VMEM)
     smem = pl.BlockSpec(memory_space=pltpu.SMEM)
+    whole = pl.BlockSpec(memory_space=pl.ANY)
     bf16, f32 = jnp.bfloat16, jnp.float32
     dma = pltpu.SemaphoreType.DMA
     pads = inner // 128 + 2 * groups
     return pl.pallas_call(
         functools.partial(relay_kernel, sizes),
         out_shape=jax.ShapeDtypeStruct(micro_in.shape, bf16),
-        in_specs=[vmem] * 7 + [smem] * 3 + [vmem] * 4,
+        in_specs=[vmem] * 2 + [whole] * 4 + [vmem] + [smem] * 3 + [vmem] * 3 + [whole],
         out_specs=vmem,
         scratch_shapes=[
-            pltpu.VMEM((micro, owners, sections, share, block), bf16),
+            pltpu.VMEM((inner, width), bf16),
+            pltpu.VMEM((inner, width), bf16),
+            pltpu.VMEM((2, width * groups, state), bf16),
+            pltpu.VMEM((2, width, groups * state), bf16),
+            pltpu.VMEM((inner, width), bf16),
+            pltpu.VMEM((micro, ring, sections, share, block), bf16),
             pltpu.VMEM((micro, owners, length, block), bf16),
-            pltpu.VMEM((micro, owners, length, block), bf16),
-            pltpu.VMEM((micro, owners, length, block), bf16),
+            pltpu.VMEM((micro, cores - 1, ring, length, block), bf16),
+            pltpu.VMEM((micro, cores - 1, ring, length, block), bf16),
+            pltpu.VMEM((micro, ring, length, block), f32),
+            pltpu.VMEM((micro, ring, length, block), bf16),
+            pltpu.VMEM((micro, ring, length, block), bf16),
             pltpu.VMEM((micro, length, block), bf16),
             pltpu.VMEM((micro, sections, share, block), bf16),
             pltpu.VMEM((micro, share, block), bf16),
-            pltpu.VMEM((micro, 8, 128), f32),
-            pltpu.VMEM((micro, owners, 8, 128), f32),
+            pltpu.VMEM((micro, 1, 128), f32),
+            pltpu.VMEM((micro, owners, 1, 128), f32),
             pltpu.VMEM((micro, 128, 128), f32),
             pltpu.VMEM((pads, length + 16, 128), f32),
-            dma((micro, owners)),
-            dma((micro, owners, sections)),
-            dma((micro, owners - 1)),
-            dma((micro, owners)),
+            dma((5,)),
+            dma((micro, ring)),
+            dma((micro, ring, sections)),
+            dma((micro, cores - 1, ring)),
+            dma((micro, cores - 1, ring)),
+            dma((micro, ring - 1)),
+            dma((micro, ring)),
             dma((micro, ring)),
             dma((micro, owners)),
             dma((micro, ring, cores - 1)),
@@ -719,7 +818,7 @@
     sizes = dict(mesh.shape)
 
     def chosen(micro_in, *weights):
-        fits = micro_in.shape[2] % 128 == 0 and micro_in.shape[1] % 8 == 0
+        fits = micro_in.shape[2] % 128 == 0 and micro_in.shape[1] % 8 == 0 and 256 % weights[3].shape[2] == 0 and weights[3].shape[3] == 128
         return (fused_body if fits else body)(micro_in, *weights, *(() if not fits else (sizes,)))
 
     return jax.shard_map(

time: 89.6 us -> 78.5 us (0.88)
  Pallas kernels: 83.4 us -> 76.9 us
  local copies, waits for them, and re-layouts: 5.86 us -> 1.31 us
    pallas_call x1, Pallas kernels: 83.4 us -> 76.9 us  [fused_body(): pl.pallas_call(functools.partial(relay_kernel, sizes), out_shape=jax.Shap...]
    another operation x1 -> x0, local copies, waits for them, and re-layouts: 3.22 us -> none  [fused_body(): proj_read[0].reshape(width, groups * state)]
    unnamed x3 -> x1, local copies, waits for them, and re-layouts: 2.03 us -> 1.31 us
where the time goes in v2:
time: 78.5 us; the launch traced here: 78.2 us
  Pallas kernels  76.9 us (98%)
  local copies, waits for them, and re-layouts  1.31 us (2%)
    pallas_call x1, Pallas kernels, fused_body(): pl.pallas_call(functools.partial(relay_kernel, sizes), out_shape=jax.Shap...  76.9 us

profile of v2, /device:TPU:0, one launch (start us, length us, event | category | flops | bytes accessed | tf_op | source)
XLA Modules:
  0.0 78.2 jit_solution(15894049667167300849)
XLA Ops:
  0.0 76.9 %shard_map.136 = bf16[2,24,128]{2,1,0:T(8,128)(2,1)} custom-call(bf16[2,24,128]{2,1,0:T(8,128)(2,1)} %in_ref.1, f32[1,1024]{1,0:T(1,128)} %gain_ref.1, bf16[256,1024]{1,0:T(8,128)(2,1)} %bitcast.26, bf16[256,1024]{1,0:T(8,128)(2,1)} %bitcast.27, bf16[4096,128]{1,0:T(8,128)(2,1)} %bitcast.24, bf16[4096,128]{1,0:T(8,128)(2,1)} %bitcast.25, ...), custom_call_target="tpu_custom_call" | custom-call | tf_op jit(solution)/shard_map/pallas_call | solution.py:772
  76.9 1.3 %copy.16 = bf16[2,24,128]{2,1,0:T(8,128)(2,1)} copy(bf16[2,24,128]{2,1,0:T(8,128)(2,1)} %shard_map.136) | data formatting | bytes 24576

commit v3 on v2

--- a/solution.py
+++ b/solution.py
@@ -685,12 +685,15 @@
         own = column[m, pl.ds(pl.multiple_of(s * share, 8), share), :]
         out_ref[m] = (final_in[m].astype(jnp.float32) * own).astype(jnp.bfloat16)
 
-    for m in range(micro):
+    receive(0)
+    mix(0)
+    send_pairs(0)
+    for m in range(1, micro):
         receive(m)
         mix(m)
+        reduce(m - 1)
         send_pairs(m)
-    for m in range(micro):
-        reduce(m)
+    reduce(micro - 1)
     for m in range(micro):
         finish(m)
 

time: 78.5 us -> 75.5 us (0.962)
  Pallas kernels: 76.9 us -> 73.9 us
    pallas_call x1, Pallas kernels: 76.9 us -> 73.9 us  [fused_body(): pl.pallas_call(functools.partial(relay_kernel, sizes), out_shape=jax.Shap...]
where the time goes in v3:
time: 75.5 us; the launch traced here: 75.2 us
  Pallas kernels  73.9 us (98%)
  local copies, waits for them, and re-layouts  1.31 us (2%)
    pallas_call x1, Pallas kernels, fused_body(): pl.pallas_call(functools.partial(relay_kernel, sizes), out_shape=jax.Shap...  73.9 us

profile of v3, /device:TPU:0, one launch (start us, length us, event | category | flops | bytes accessed | tf_op | source)
XLA Modules:
  0.0 75.2 jit_solution(10662249045272765728)
XLA Ops:
  0.0 73.9 %shard_map.136 = bf16[2,24,128]{2,1,0:T(8,128)(2,1)} custom-call(bf16[2,24,128]{2,1,0:T(8,128)(2,1)} %in_ref.1, f32[1,1024]{1,0:T(1,128)} %gain_ref.1, bf16[256,1024]{1,0:T(8,128)(2,1)} %bitcast.26, bf16[256,1024]{1,0:T(8,128)(2,1)} %bitcast.27, bf16[4096,128]{1,0:T(8,128)(2,1)} %bitcast.24, bf16[4096,128]{1,0:T(8,128)(2,1)} %bitcast.25, ...), custom_call_target="tpu_custom_call" | custom-call | tf_op jit(solution)/shard_map/pallas_call | solution.py:775
  73.9 1.3 %copy.16 = bf16[2,24,128]{2,1,0:T(8,128)(2,1)} copy(bf16[2,24,128]{2,1,0:T(8,128)(2,1)} %shard_map.136) | data formatting | bytes 24576

commit v4 on v3

--- a/solution.py
+++ b/solution.py
@@ -462,10 +462,29 @@
 
             for twin in range(1, cores):
                 twin_copy(m, zz, twin).start()
+        sums = half_dots(m, c)
         for twin in range(1, cores):
             other = lax.rem(c + twin, cores)
             for step in range(ring):
                 wait_block(m, other * ring + lax.rem(z + step, ring))
+            sums = [old + new for old, new in zip(sums, half_dots(m, other))]
+        return sums
+
+    def half_dots(m, core):
+        span = ring * block
+        columns = pl.ds(pl.multiple_of(core * span, 128), span)
+        x = jnp.concatenate(
+            [acts[m, core * ring + zz].astype(jnp.float32) for zz in range(ring)], axis=1
+        )
+        scaled = (x * gain_ref[:, columns]).astype(jnp.bfloat16)
+        return [
+            jnp.sum(x * x, axis=1, keepdims=True),
+            *[matmul(step_w[d, :, columns], scaled, NT_DIMS) for d in range(2)],
+            matmul(scaled, value_w[:, columns], NT_DIMS),
+            matmul(scaled, mixed_w[0, columns, :]),
+            matmul(scaled, mixed_w[1, columns, :]),
+            matmul(scaled, gate_w[:, columns], NT_DIMS),
+        ]
 
     def pre_copy(m, twin, zz):
         other = lax.rem(c + twin, cores)
@@ -487,23 +506,13 @@
             {"pp": s, "fs": zz, "tp": c},
         )
 
-    def mix(m):
-        x = [acts[m, k].astype(jnp.float32) for k in range(owners)]
-        total = x[0] * x[0]
-        for k in range(1, owners):
-            total = total + x[k] * x[k]
-        scale = lax.rsqrt(jnp.sum(total, axis=1, keepdims=True) / width + epsilon)
-        normed = jnp.concatenate(
-            [
-                (x[k] * scale * gain_ref[:, k * block : (k + 1) * block]).astype(jnp.bfloat16)
-                for k in range(owners)
-            ],
-            axis=1,
-        )
-        step_row = (
-            jnp.concatenate([matmul(step_w[d], normed, NT_DIMS) for d in range(2)], axis=0)
-            + bias_col
-        )
+    def mix(m, sums):
+        squared, step_f, step_b, value_raw, write_raw, read_raw, gate_raw = sums
+        scale = lax.rsqrt(squared / width + epsilon)
+        scale_row = jnp.sum(jnp.where(diag, scale, 0.0), axis=0, keepdims=True)
+        step_row = jnp.concatenate([step_f, step_b], axis=0) * scale_row + bias_col
+        value_raw, write_raw = value_raw * scale, write_raw * scale
+        read_raw, gate_raw = read_raw * scale, gate_raw * scale
         dt = jnp.maximum(step_row, 0.0) + jnp.log1p(jnp.exp(-jnp.abs(step_row)))
         a = dt * decay_col
         high = lax.Precision.HIGHEST
@@ -511,10 +520,6 @@
         bwd_row = matmul(a, tri_up, NT_DIMS, high)
         fwd_col = matmul(tri_low, a, NT_DIMS, high)
         bwd_col = matmul(tri_up, a, NT_DIMS, high)
-        value_raw = matmul(normed, value_w[...], NT_DIMS)
-        write_raw = matmul(normed, mixed_w[0])
-        read_raw = matmul(normed, mixed_w[1])
-        gate_raw = matmul(normed, gate_w[...], NT_DIMS)
         pieces = inner // 128
         value = jnp.concatenate(
             [
@@ -685,12 +690,10 @@
         own = column[m, pl.ds(pl.multiple_of(s * share, 8), share), :]
         out_ref[m] = (final_in[m].astype(jnp.float32) * own).astype(jnp.bfloat16)
 
-    receive(0)
-    mix(0)
+    mix(0, receive(0))
     send_pairs(0)
     for m in range(1, micro):
-        receive(m)
-        mix(m)
+        mix(m, receive(m))
         reduce(m - 1)
         send_pairs(m)
     reduce(micro - 1)

time: 75.5 us -> 73.7 us (0.976)
  Pallas kernels: 73.9 us -> 72.1 us
    pallas_call x1, Pallas kernels: 73.9 us -> 72.1 us  [fused_body(): pl.pallas_call(functools.partial(relay_kernel, sizes), out_shape=jax.Shap...]
where the time goes in v4:
time: 73.7 us; the launch traced here: 73.4 us
  Pallas kernels  72.1 us (98%)
  local copies, waits for them, and re-layouts  1.31 us (2%)
    pallas_call x1, Pallas kernels, fused_body(): pl.pallas_call(functools.partial(relay_kernel, sizes), out_shape=jax.Shap...  72.1 us

profile of v4, /device:TPU:0, one launch (start us, length us, event | category | flops | bytes accessed | tf_op | source)
XLA Modules:
  0.0 73.4 jit_solution(3288361723228214384)
XLA Ops:
  0.0 72.1 %shard_map.136 = bf16[2,24,128]{2,1,0:T(8,128)(2,1)} custom-call(bf16[2,24,128]{2,1,0:T(8,128)(2,1)} %in_ref.1, f32[1,1024]{1,0:T(1,128)} %gain_ref.1, bf16[256,1024]{1,0:T(8,128)(2,1)} %bitcast.26, bf16[256,1024]{1,0:T(8,128)(2,1)} %bitcast.27, bf16[4096,128]{1,0:T(8,128)(2,1)} %bitcast.24, bf16[4096,128]{1,0:T(8,128)(2,1)} %bitcast.25, ...), custom_call_target="tpu_custom_call" | custom-call | tf_op jit(solution)/shard_map/pallas_call | solution.py:778
  72.1 1.3 %copy.16 = bf16[2,24,128]{2,1,0:T(8,128)(2,1)} copy(bf16[2,24,128]{2,1,0:T(8,128)(2,1)} %shard_map.136) | data formatting | bytes 24576
